TPU v7x, 32 devices: a whole 2x2x4 slice. The times are simulated.
32 devices in a mesh: ep: 8 (over z, x), tp: 4 (over y, core).
Axes of the slice: x: 2, y: 2, z: 4, core: 2. Of those that a mesh axis runs over, the one named last changes fastest.
Arguments:
- resid: bfloat16 [256, 2048], P('ep'), may hold values from -6 to 6
- norm_gain: bfloat16 [2048], replicated, may hold values from 0.099609375 to 1.8984375
- w_query: bfloat16 [2048, 1024], P(None, 'tp'), may hold values from -0.125 to 0.125
- w_key: bfloat16 [2048, 1024], P(None, 'tp'), may hold values from -0.125 to 0.125
- w_value: bfloat16 [2048, 1024], P(None, 'tp'), may hold values from -0.125 to 0.125
- w_gate: bfloat16 [2048, 1024], P(None, 'tp'), may hold values from -0.125 to 0.125
- head_gain: bfloat16 [1024], P('tp'), may hold values from 0.099609375 to 1.8984375
- w_output: bfloat16 [1024, 2048], P('tp'), may hold values from -0.1875 to 0.1875
- state: float32 [256, 8, 128, 128], P('ep', 'tp'), may hold values from -0.6 to 0.6
- positions: int32 [256], P('ep'), may hold values from 1024 to 8191
- ffn_gain: bfloat16 [2048], replicated, may hold values from 0.099609375 to 1.8984375
- w_mix: bfloat16 [2048], replicated, may hold values from -0.125 to 0.125
- dense_gate: bfloat16 [2048, 5632], P('tp', 'ep'), may hold values from -0.125 to 0.125
- dense_up: bfloat16 [2048, 5632], P('tp', 'ep'), may hold values from -0.125 to 0.125
- dense_down: bfloat16 [5632, 2048], P('ep', 'tp'), may hold values from -0.109375 to 0.109375
- routes: int32 [256, 2], P('ep'), may hold values from 0 to 7, all different within a row; in each aligned block of 32 rows (0 to 31, 32 to 63, ...) at most 16 rows name the same one
- route_weight: bfloat16 [256, 2], P('ep'), may hold values from 0.19921875 to 1
- expert_gate: bfloat16 [8, 2048, 4096], P('ep', None, 'tp'), may hold values from -0.125 to 0.125
- expert_up: bfloat16 [8, 2048, 4096], P('ep', None, 'tp'), may hold values from -0.125 to 0.125
- expert_down: bfloat16 [8, 4096, 2048], P('ep', 'tp'), may hold values from -0.09375 to 0.09375
Outputs:
- final: bfloat16 [256, 2048], P('ep', 'tp')
- new_state: float32 [256, 8, 128, 128], P('ep', 'tp')
Inputs may be any that keep to these rules, and one draw needn't show every extreme that they name: `routes`: each row names 2 different experts; in the rows of one index of ep no expert is named by more than 16 rows, a bound that some block reaches; every expert is named by some row.
All inputs are finite; a program needn't handle non-finite values.
Results may differ from a plain program's by a relative error of at most 0.018.
Values may be sent and summed in bfloat16 or wider, within the bound.
A program may use at most 64 MiB of HBM per device.

v0:
```python
import jax
import jax.numpy as jnp
from jax import lax
from jax.sharding import PartitionSpec as P

EPSILON = 1e-06
THETA = 10000.0


def rms_norm(inputs, scaling):
    square = jnp.mean(inputs * inputs, axis=-1, keepdims=True)
    return inputs * lax.rsqrt(square + EPSILON) * scaling.astype(jnp.float32)


def rotate(inputs, places):
    halfway = inputs.shape[-1] // 2
    inverse = THETA ** (-jnp.arange(halfway, dtype=jnp.float32) / halfway)
    angles = places.astype(jnp.float32)[:, None] * inverse[None, :]
    cosine = jnp.cos(angles)[:, None, :]
    sine_of = jnp.sin(angles)[:, None, :]
    former = inputs[..., :halfway]
    latter = inputs[..., halfway:]
    return jnp.concatenate(
        [former * cosine - latter * sine_of, former * sine_of + latter * cosine], axis=-1
    )


def retain(queries, keys_in, values_in, gating, memory, places, head_first, head_gain):
    seqs_here = queries.shape[0]
    heads_here = memory.shape[1]
    head_size = memory.shape[2]
    head_shape = (seqs_here, heads_here, head_size)
    query_rot = rotate(queries.astype(jnp.float32).reshape(head_shape), places)
    key_rot = rotate(keys_in.astype(jnp.float32).reshape(head_shape), places) * head_size ** (-0.5)
    value_heads = values_in.astype(jnp.float32).reshape(head_shape)
    head_index = head_first + jnp.arange(heads_here, dtype=jnp.float32)
    decays = 1.0 - jnp.exp2(-1.0 - 1.5 * head_index)
    within = jnp.sum(query_rot * key_rot, axis=-1, keepdims=True) * value_heads
    carried = (
        jnp.einsum("shd,shde->she", query_rot, memory, precision=lax.Precision.HIGHEST)
        * decays[None, :, None]
    )
    mixture = within + carried
    new_memory = (
        decays[None, :, None, None] * memory + key_rot[:, :, :, None] * value_heads[:, :, None, :]
    )
    centre = jnp.mean(mixture, axis=-1, keepdims=True)
    spread = jnp.mean(jnp.square(mixture - centre), axis=-1, keepdims=True)
    normed = ((mixture - centre) * lax.rsqrt(spread + EPSILON)).reshape(
        seqs_here, heads_here * head_size
    )
    normed = normed * head_gain.astype(jnp.float32)
    output = (jax.nn.silu(gating.astype(jnp.float32)) * normed).astype(jnp.bfloat16)
    return (output, new_memory)


def expert_hidden(chosen, gate_weight, up_weight):
    gate_value = jnp.dot(chosen, gate_weight, preferred_element_type=jnp.float32)
    up_value = jnp.dot(chosen, up_weight, preferred_element_type=jnp.float32)
    return (jax.nn.silu(gate_value) * up_value).astype(jnp.bfloat16)


def padded_experts(
    normed_mid, routes, route_weight, expert_gate, expert_up, expert_down, capacity, experts_all
):
    seq_dev, model_width = normed_mid.shape
    top_count = routes.shape[1]
    flat_ids = routes.reshape(-1)
    expert_ids = jnp.arange(experts_all, dtype=jnp.int32)
    onehot = (flat_ids[:, None] == expert_ids[None, :]).astype(jnp.int32)
    ranks = jnp.sum((jnp.cumsum(onehot, axis=0) - 1) * onehot, axis=1)
    slot_ids = flat_ids * capacity + ranks
    slot_range = jnp.arange(experts_all * capacity, dtype=jnp.int32)
    dispatch = (slot_range[:, None] == slot_ids[None, :]).astype(jnp.bfloat16)
    repeated = jnp.repeat(normed_mid, top_count, axis=0)
    outgoing = jnp.dot(dispatch, repeated, preferred_element_type=jnp.float32).astype(jnp.bfloat16)
    outgoing = outgoing.reshape(experts_all, capacity, model_width)
    arrived = lax.all_to_all(outgoing, "ep", split_axis=0, concat_axis=0, tiled=True)
    sources = arrived.shape[0]
    items = arrived.shape[1]
    hidden_e = expert_hidden(
        arrived.reshape(sources * items, model_width), expert_gate[0], expert_up[0]
    )
    partial_value = jnp.dot(hidden_e, expert_down[0], preferred_element_type=jnp.float32)
    summed = lax.psum_scatter(
        partial_value.astype(jnp.bfloat16), "tp", scatter_dimension=1, tiled=True
    )
    returned = lax.all_to_all(
        summed.reshape(sources, items, summed.shape[1]),
        "ep",
        split_axis=0,
        concat_axis=0,
        tiled=True,
    )
    flat_back = returned.reshape(experts_all * capacity, returned.shape[2])
    weighted = flat_back[slot_ids].astype(jnp.float32) * route_weight.reshape(-1)[:, None].astype(
        jnp.float32
    )
    return jnp.sum(weighted.reshape(seq_dev, top_count, weighted.shape[1]), axis=1)


def per_device(
    resid,
    norm_gain,
    w_query,
    w_key,
    w_value,
    w_gate,
    head_gain,
    w_output,
    state,
    positions,
    ffn_gain,
    w_mix,
    dense_gate,
    dense_up,
    dense_down,
    routes,
    route_weight,
    expert_gate,
    expert_up,
    expert_down,
):
    seq_dev = resid.shape[0]
    model_width = resid.shape[1]
    tp_count = lax.axis_size("tp")
    ep_count = lax.axis_size("ep")
    model_tp = model_width // tp_count
    tp_index = lax.axis_index("tp")
    normed_in = rms_norm(resid.astype(jnp.float32), norm_gain).astype(jnp.bfloat16)

    def project(weight):
        return jnp.dot(normed_in, weight, preferred_element_type=jnp.float32).astype(jnp.bfloat16)

    heads_here = state.shape[1]
    head_first = (tp_index * heads_here).astype(jnp.float32)
    retained, new_state = retain(
        project(w_query),
        project(w_key),
        project(w_value),
        project(w_gate),
        state,
        positions,
        head_first,
        head_gain,
    )
    partial_value = jnp.dot(retained, w_output, preferred_element_type=jnp.float32)
    attention = lax.psum(partial_value.astype(jnp.bfloat16), "tp").astype(jnp.float32)
    middle = resid.astype(jnp.float32) + attention
    normed_mid = rms_norm(middle, ffn_gain).astype(jnp.bfloat16)
    mixing = jax.nn.sigmoid(jnp.dot(normed_mid, w_mix[:, None], preferred_element_type=jnp.float32))

    def own_columns(matrix):
        return lax.dynamic_slice_in_dim(matrix, tp_index * model_tp, model_tp, 1)

    top_count = routes.shape[1]
    capacity = max(2, 2 * seq_dev * top_count // ep_count)
    dense_rows = lax.all_gather(own_columns(normed_mid), "ep", axis=0, tiled=True)
    moe_out = padded_experts(
        normed_mid, routes, route_weight, expert_gate, expert_up, expert_down, capacity, ep_count
    )
    gate_part = jnp.dot(dense_rows, dense_gate, preferred_element_type=jnp.float32)
    up_part = jnp.dot(dense_rows, dense_up, preferred_element_type=jnp.float32)
    gate_sum, up_sum = (
        lax.psum(gate_part.astype(jnp.bfloat16), "tp").astype(jnp.float32),
        lax.psum(up_part.astype(jnp.bfloat16), "tp").astype(jnp.float32),
    )
    dense_hidden = (jax.nn.silu(gate_sum) * up_sum).astype(jnp.bfloat16)
    dense_out = lax.psum_scatter(
        jnp.dot(dense_hidden, dense_down, preferred_element_type=jnp.float32).astype(jnp.bfloat16),
        "ep",
        scatter_dimension=0,
        tiled=True,
    ).astype(jnp.float32)
    final = (own_columns(middle) + moe_out + mixing * dense_out).astype(jnp.bfloat16)
    return (final, new_state)


def solution(mesh):
    in_specs = (
        P("ep", None),
        P(),
        P(None, "tp"),
        P(None, "tp"),
        P(None, "tp"),
        P(None, "tp"),
        P("tp"),
        P("tp", None),
        P("ep", "tp", None, None),
        P("ep"),
        P(),
        P(),
        P("tp", "ep"),
        P("tp", "ep"),
        P("ep", "tp"),
        P("ep", None),
        P("ep", None),
        P("ep", None, "tp"),
        P("ep", None, "tp"),
        P("ep", "tp", None),
    )
    out_specs = (P("ep", "tp"), P("ep", "tp", None, None))
    return jax.shard_map(
        per_device, mesh=mesh, in_specs=in_specs, out_specs=out_specs, check_vma=False
    )
```

profile of v0, /device:TPU:0, one launch (start us, length us, event | category | flops | bytes accessed | tf_op | source)
XLA Modules:
  0.0 234.7 jit_solution(9448984096883275482)
XLA Ops:
  8.0 1.0 fusion.40
  10.4 1.6 fusion.20
  12.1 1.7 fusion.19
  13.8 1.6 fusion.18
  16.0 5.3 %fusion.61 = f32[32,2,1,128]{3,2,1,0:T(1,128)S(1)} fusion(f32[32,2,128,1]{2,3,1,0:T(1,128)S(1)} %bitcast.72, f32[32,2,128,128]{3,2,1,0:T(8,128)} %param.28), kind=kOutput, calls=%fused_computation.95 | convolution fusion | flops 12582912 | bytes 4259840 | tf_op jit(solution)/shard_map/shd,shde->she/dot_general | solution.py:40
  21.9 1.5 convolution_convert_fusion.1
  24.0 34.1 %all-reduce.4.cloned.1.call-done = bf16[32,2048]{1,0:T(8,128)(2,1)} async-done(((bf16[32,2048]{1,0:T(8,128)(2,1)}), bf16[32,2048]{1,0:T(8,128)(2,1)}) %all-reduce.4.cloned.1.call-update) | async-done | bytes 131088 | tf_op jit(solution)/shard_map/psum | solution.py:148
  58.1 1.1 convert_add_fusion
  59.1 1.0 multiply_convert_fusion
  60.4 1.1 convolution_convert_fusion
  61.5 5.5 %all-to-all-start = ((bf16[8,16,2048]{2,1,0:T(8,128)(2,1)}), bf16[8,16,2048]{2,1,0:T(8,128)(2,1)S(1)}, u32[]{:S(2)}, u32[]{:S(2)}) async-start(bf16[8,16,2048]{2,1,0:T(8,128)(2,1)} %bitcast.4), calls=%async_computation | async-start | bytes 1048576 | tf_op jit(solution)/shard_map/all_to_all | solution.py:78
  67.0 36.6 %all_gather.3 = bf16[256,512]{1,0:T(8,128)(2,1)S(1)} all-gather(bf16[32,512]{1,0:T(8,128)(2,1)S(1)} %constant_dynamic-slice_fusion), channel_id=1, replica_groups=mesh['ep'=8,'tp'=4] {'ep'}, dimensions={0}, use_global_device_ids=true | all-gather | bytes 294912 | tf_op jit(solution)/shard_map/all_gather | solution.py:158
  103.7 1.1 convolution_convert_fusion.2
  104.8 1.1 convolution_convert_fusion.3
  106.0 2.9 %fusion.5 = f32[128,1024]{1,0:T(8,128)S(1)} fusion(bf16[128,2048]{1,0:T(8,128)(2,1)S(1)} %bitcast.69, bf16[1,2048,1024]{2,1,0:T(8,128)(2,1)} %param.37), kind=kOutput, calls=%fused_computation.6 | convolution fusion | flops 536870912 | bytes 5242880 | tf_op jit(solution)/shard_map/dot_general | solution.py:58
  109.0 5.6 %fusion.7 = bf16[128,2048]{1,0:T(8,128)(2,1)} fusion(bf16[1,1024,2048]{2,1,0:T(8,128)(2,1)} %param.39, bf16[128,2048]{1,0:T(8,128)(2,1)S(1)} %bitcast.70, bf16[1,2048,1024]{2,1,0:T(8,128)(2,1)} %param.38, f32[128,1024]{1,0:T(8,128)S(1)} %fusion.5), kind=kOutput, calls=%fused_computation.9 | convolution fusion | flops 1074790400 | bytes 9961472 | tf_op jit(solution)/shard_map/dot_general | solution.py:84
  114.9 4.3 %multiply_add_fusion = f32[32,2,128,128]{3,2,1,0:T(8,128)} fusion(f32[32,2,128,128]{3,2,1,0:T(8,128)} %param.28, f32[32,2,128]{2,1,0:T(2,128)S(1)} %copy-done.6, f32[32,2,128]{2,1,0:T(2,128)S(1)} %copy-done.8, f32[2]{0:T(128)S(1)} %exponential_subtract_fusion), kind=kLoop, calls=%fused_computation.8 | loop fusion | flops 3145728 | bytes 8454152 | tf_op jit(solution)/shard_map/add | solution.py:45
  119.2 18.0 %all-reduce.6.cloned.1.call-done = (bf16[256,704]{0,1:T(8,128)(2,1)}, bf16[256,704]{0,1:T(8,128)(2,1)}) async-done(((bf16[256,704]{0,1:T(8,128)(2,1)}, bf16[256,704]{0,1:T(8,128)(2,1)}), (bf16[256,704]{0,1:T(8,128)(2,1)}, bf16[256,704]{0,1:T(8,128)(2,1)})) %all-reduce.6.cloned.1.call-update) | async-done | bytes 720912 | tf_op jit(solution)/shard_map/psum | solution.py:166
  137.2 2.2 convolution_convert_fusion.4
  139.5 21.9 %reduce-scatter.3.cloned.1.call-done = bf16[128,512]{1,0:T(8,128)(2,1)} async-done(((bf16[128,2048]{1,0:T(8,128)(2,1)}), bf16[128,512]{1,0:T(8,128)(2,1)}) %reduce-scatter.3.cloned.1.call-update) | async-done | bytes 131088 | tf_op jit(solution)/shard_map/reduce_scatter | solution.py:85
  161.4 5.5 %all-to-all-start.1 = ((bf16[8,16,512]{2,1,0:T(8,128)(2,1)}), bf16[8,16,512]{2,1,0:T(8,128)(2,1)S(1)}, u32[]{:S(2)}, u32[]{:S(2)}) async-start(bf16[8,16,512]{2,1,0:T(8,128)(2,1)} %bitcast.73), calls=%async_computation.2 | async-start | bytes 262144 | tf_op jit(solution)/shard_map/all_to_all | solution.py:88
  167.2 7.1 %all-to-all-done.1 = bf16[8,16,512]{2,1,0:T(8,128)(2,1)S(1)} async-done(((bf16[8,16,512]{2,1,0:T(8,128)(2,1)}), bf16[8,16,512]{2,1,0:T(8,128)(2,1)S(1)}, u32[]{:S(2)}, u32[]{:S(2)}) %all-to-all-start.1) | async-done | bytes 131104 | tf_op jit(solution)/shard_map/all_to_all | solution.py:88
  175.3 51.4 %reduce-scatter.5.cloned.1.call-done = bf16[32,512]{1,0:T(8,128)(2,1)} async-done(((bf16[256,512]{1,0:T(8,128)(2,1)}), bf16[32,512]{1,0:T(8,128)(2,1)}) %reduce-scatter.5.cloned.1.call-update) | async-done | bytes 32784 | tf_op jit(solution)/shard_map/reduce_scatter | solution.py:169
  226.7 1.4 add_convert_fusion
  (76 shorter events, 5.8 us)
Async XLA Ops:
  7.2 14.7 %copy-start = (bf16[256,2048]{1,0:T(8,128)(2,1)S(1)}, bf16[256,2048]{1,0:T(8,128)(2,1)}, u32[]{:S(2)}) copy-start(bf16[256,2048]{1,0:T(8,128)(2,1)} %param.27) | copy-start | bytes 3145732
  7.2 50.9 %all-reduce.4.cloned.1.call-start = ((), (), s32[]{:S(2)}) async-start(), calls=%async_computation.4 | async-start | bytes 262144 | tf_op jit(solution)/shard_map/psum | solution.py:148
  12.0 9.9 %copy-start.1 = (bf16[32,2048]{1,0:T(8,128)(2,1)S(1)}, bf16[32,2048]{1,0:T(8,128)(2,1)}, u32[]{:S(2)}) copy-start(bf16[32,2048]{1,0:T(8,128)(2,1)} %param.20) | copy-start | bytes 393220
  12.0 9.9 %copy-start.2 = (bf16[2048,256]{1,0:T(8,128)(2,1)S(1)}, bf16[2048,256]{1,0:T(8,128)(2,1)}, u32[]{:S(2)}) copy-start(bf16[2048,256]{1,0:T(8,128)(2,1)} %param.25) | copy-start | bytes 3145732
  15.4 8.0 %copy-start.11 = (s32[32,2]{0,1:T(2,128)S(1)}, s32[32,2]{0,1:T(2,128)}, u32[]{:S(2)}) copy-start(s32[32,2]{0,1:T(2,128)} %param.35) | copy-start | bytes 772
  15.5 8.5 %copy-start.9 = (bf16[2048]{0:T(1024)(128)(2,1)S(1)}, bf16[2048]{0:T(1024)(128)(2,1)}, u32[]{:S(2)}) copy-start(bf16[2048]{0:T(1024)(128)(2,1)} %param.30) | copy-start | bytes 12292
  15.5 6.0 %copy-start.5 = (f32[32,2,128]{2,1,0:T(2,128)}, f32[32,2,128]{2,1,0:T(2,128)S(1)}, u32[]{:S(2)}) copy-start(f32[32,2,128]{2,1,0:T(2,128)S(1)} %reshape.238) | copy-start | bytes 98308
  16.0 5.9 %copy-start.7 = (f32[32,2,128]{2,1,0:T(2,128)}, f32[32,2,128]{2,1,0:T(2,128)S(1)}, u32[]{:S(2)}) copy-start(f32[32,2,128]{2,1,0:T(2,128)S(1)} %get-tuple-element.17) | copy-start | bytes 98308
  21.3 82.4 %copy-start.3 = (bf16[512,704]{0,1:T(8,128)(2,1)S(1)}, bf16[512,704]{0,1:T(8,128)(2,1)}, u32[]{:S(2)}) copy-start(bf16[512,704]{0,1:T(8,128)(2,1)} %param.33) | copy-start | bytes 2162692
  23.4 81.5 %copy-start.4 = (bf16[512,704]{0,1:T(8,128)(2,1)S(1)}, bf16[512,704]{0,1:T(8,128)(2,1)}, u32[]{:S(2)}) copy-start(bf16[512,704]{0,1:T(8,128)(2,1)} %param.32) | copy-start | bytes 2162692
  61.5 44.6 %all-to-all-start = ((bf16[8,16,2048]{2,1,0:T(8,128)(2,1)}), bf16[8,16,2048]{2,1,0:T(8,128)(2,1)S(1)}, u32[]{:S(2)}, u32[]{:S(2)}) async-start(bf16[8,16,2048]{2,1,0:T(8,128)(2,1)} %bitcast.4), calls=%async_computation | async-start | bytes 1048576 | tf_op jit(solution)/shard_map/all_to_all | solution.py:78
  67.0 70.2 %all-reduce.6.cloned.1.call-start = ((), (), s32[]{:S(2)}) async-start(), calls=%async_computation.7 | async-start | bytes 1441792 | tf_op jit(solution)/shard_map/psum | solution.py:166
  106.0 55.4 %reduce-scatter.3.cloned.1.call-start = ((), (), s32[]{:S(2)}) async-start(), calls=%async_computation.5 | async-start | bytes 655360 | tf_op jit(solution)/shard_map/reduce_scatter | solution.py:85
  109.0 5.9 %copy-start.6 = (f32[32,2,128]{2,1,0:T(2,128)S(1)}, f32[32,2,128]{2,1,0:T(2,128)}, u32[]{:S(2)}) copy-start(f32[32,2,128]{2,1,0:T(2,128)} %copy-done.5) | copy-start | bytes 98308
  109.0 5.9 %copy-start.8 = (f32[32,2,128]{2,1,0:T(2,128)S(1)}, f32[32,2,128]{2,1,0:T(2,128)}, u32[]{:S(2)}) copy-start(f32[32,2,128]{2,1,0:T(2,128)} %copy-done.7) | copy-start | bytes 98308
  114.6 112.0 %reduce-scatter.5.cloned.1.call-start = ((), (), s32[]{:S(2)}) async-start(), calls=%async_computation.6 | async-start | bytes 294912 | tf_op jit(solution)/shard_map/reduce_scatter | solution.py:169
  114.9 22.3 %copy-start.13 = (bf16[704,512]{1,0:T(8,128)(2,1)S(1)}, bf16[704,512]{1,0:T(8,128)(2,1)}, u32[]{:S(2)}) copy-start(bf16[704,512]{1,0:T(8,128)(2,1)} %param.34) | copy-start | bytes 2162692
  119.2 47.7 %copy-start.10 = (bf16[2048]{0:T(1024)(128)(2,1)S(1)}, bf16[2048]{0:T(1024)(128)(2,1)}, u32[]{:S(2)}) copy-start(bf16[2048]{0:T(1024)(128)(2,1)} %param.31) | copy-start | bytes 12292
  119.2 47.7 %copy-start.12 = (bf16[32,2]{0,1:T(2,128)(2,1)S(1)}, bf16[32,2]{0,1:T(2,128)(2,1)}, u32[]{:S(2)}) copy-start(bf16[32,2]{0,1:T(2,128)(2,1)} %param.36) | copy-start | bytes 388
  161.4 12.9 %all-to-all-start.1 = ((bf16[8,16,512]{2,1,0:T(8,128)(2,1)}), bf16[8,16,512]{2,1,0:T(8,128)(2,1)S(1)}, u32[]{:S(2)}, u32[]{:S(2)}) async-start(bf16[8,16,512]{2,1,0:T(8,128)(2,1)} %bitcast.73), calls=%async_computation.2 | async-start | bytes 262144 | tf_op jit(solution)/shard_map/all_to_all | solution.py:88
Sparse Core Ops, SparseCore 0:
  23.5 34.4 all-reduce.3
  106.1 31.0 all-reduce.5
  139.7 21.6 reduce-scatter.2
  164.6 62.0 reduce-scatter.4
where the time goes:
time: 235 us
  waiting for transfers between devices  132 us (56%)
  blocking collectives  36.6 us (16%)
  matrix products  26 us (11%)
  between operations  14.2 us (6%)
  other arithmetic  12.6 us (5%)
  starting transfers between devices  11.2 us (5%)
    reduce_scatter x1, waiting for transfers between devices, per_device(): lax.psum_scatter(jnp.dot(dense_hidden, dense_down, preferred_element_type...  51.4 us
    all_gather x1, blocking collectives, per_device(): lax.all_gather(own_columns(normed_mid), 'ep', axis=0, tiled=True)  36.6 us
    psum x1, waiting for transfers between devices, per_device(): lax.psum(partial_value.astype(jnp.bfloat16), 'tp').astype(jnp.float32)  34.1 us
    reduce_scatter x1, waiting for transfers between devices, padded_experts(): lax.psum_scatter(partial_value.astype(jnp.bfloat16), 'tp', scatter_dimens...  21.9 us
    psum x1, waiting for transfers between devices, per_device(): lax.psum(up_part.astype(jnp.bfloat16), 'tp').astype(jnp.float32)  18 us
    all_to_all x1, waiting for transfers between devices, padded_experts(): lax.all_to_all(summed.reshape(sources, items, summed.shape[1]), 'ep', spl...  7.07 us
    dot_general x1, matrix products, padded_experts(): jnp.dot(hidden_e, expert_down[0], preferred_element_type=jnp.float32)  5.62 us
    all_to_all x1, starting transfers between devices, padded_experts(): lax.all_to_all(summed.reshape(sources, items, summed.shape[1]), 'ep', spl...  5.51 us
  transfers between devices with their start and end apart: 6, of which 5 were waited for; matrix products, arithmetic and copies ran while one was open for 8% of the time, Pallas kernels for 0%

commit v1 on v0

v1 whole, which is shorter than its diff:
```python
import functools

import jax
import jax.numpy as jnp
from jax import lax
from jax.experimental import pallas as pl
from jax.experimental.pallas import tpu as pltpu
from jax.sharding import PartitionSpec as P

EPSILON = 1e-06
THETA = 10000.0


def rms_norm(inputs, scaling):
    square = jnp.mean(inputs * inputs, axis=-1, keepdims=True)
    return inputs * lax.rsqrt(square + EPSILON) * scaling.astype(jnp.float32)


def rotate(inputs, places):
    halfway = inputs.shape[-1] // 2
    inverse = THETA ** (-jnp.arange(halfway, dtype=jnp.float32) / halfway)
    angles = places.astype(jnp.float32)[:, None] * inverse[None, :]
    cosine = jnp.cos(angles)[:, None, :]
    sine_of = jnp.sin(angles)[:, None, :]
    former = inputs[..., :halfway]
    latter = inputs[..., halfway:]
    return jnp.concatenate(
        [former * cosine - latter * sine_of, former * sine_of + latter * cosine], axis=-1
    )


def retain(queries, keys_in, values_in, gating, memory, places, head_first, head_gain):
    seqs_here = queries.shape[0]
    heads_here = memory.shape[1]
    head_size = memory.shape[2]
    head_shape = (seqs_here, heads_here, head_size)
    query_rot = rotate(queries.astype(jnp.float32).reshape(head_shape), places)
    key_rot = rotate(keys_in.astype(jnp.float32).reshape(head_shape), places) * head_size ** (-0.5)
    value_heads = values_in.astype(jnp.float32).reshape(head_shape)
    head_index = head_first + jnp.arange(heads_here, dtype=jnp.float32)
    decays = 1.0 - jnp.exp2(-1.0 - 1.5 * head_index)
    within = jnp.sum(query_rot * key_rot, axis=-1, keepdims=True) * value_heads
    carried = (
        jnp.einsum("shd,shde->she", query_rot, memory, precision=lax.Precision.HIGHEST)
        * decays[None, :, None]
    )
    mixture = within + carried
    new_memory = (
        decays[None, :, None, None] * memory + key_rot[:, :, :, None] * value_heads[:, :, None, :]
    )
    centre = jnp.mean(mixture, axis=-1, keepdims=True)
    spread = jnp.mean(jnp.square(mixture - centre), axis=-1, keepdims=True)
    normed = ((mixture - centre) * lax.rsqrt(spread + EPSILON)).reshape(
        seqs_here, heads_here * head_size
    )
    normed = normed * head_gain.astype(jnp.float32)
    output = (jax.nn.silu(gating.astype(jnp.float32)) * normed).astype(jnp.bfloat16)
    return (output, new_memory)


def routing(routes, route_weight, capacity, slots, experts_all):
    seq_dev, top_count = routes.shape
    flat_ids = routes.reshape(-1)
    expert_ids = jnp.arange(experts_all, dtype=jnp.int32)
    onehot = (flat_ids[:, None] == expert_ids[None, :]).astype(jnp.int32)
    ranks = jnp.sum((jnp.cumsum(onehot, axis=0) - 1) * onehot, axis=1)
    slot_ids = (flat_ids * slots + ranks).reshape(seq_dev, top_count)
    slot_range = jnp.arange(experts_all * slots, dtype=jnp.int32)
    hits = slot_ids[:, :, None] == slot_range[None, None, :]
    combine = jnp.sum(
        jnp.where(hits, route_weight.astype(jnp.float32)[:, :, None], 0.0), axis=1
    ).astype(jnp.bfloat16)
    dispatch = jnp.any(slot_range[:, None, None] == slot_ids[None, :, :], axis=2)
    dispatch = dispatch.astype(jnp.bfloat16).reshape(experts_all, slots, seq_dev)
    return dispatch, combine


def tail_kernel(
    tp_count,
    ep_count,
    slots,
    part_ref,
    resid_ref,
    gain_ref,
    mix_ref,
    dispatch_ref,
    combine_ref,
    dense_gate,
    dense_up,
    dense_down,
    expert_gate,
    expert_up,
    expert_down,
    out_ref,
    wg,
    wu,
    wd,
    eg,
    eu,
    ed,
    att_rx,
    middle,
    stat_tx,
    stat_rx,
    rows,
    hot,
    tokens,
    gu_tx,
    gu_rx,
    hidden,
    eh,
    er_tx,
    er_rx,
    do_tx,
    do_rx,
    mo_tx,
    mo_rx,
    load_sem,
    send_sem,
    recv_sem,
):
    me_t = lax.axis_index("tp")
    me_e = lax.axis_index("ep")
    seq_dev, model_width = resid_ref.shape
    width = model_width // tp_count
    block = hidden.shape[0] // tp_count
    f32 = jnp.float32
    bf16 = jnp.bfloat16

    loads = [
        pltpu.make_async_copy(source, target, load_sem.at[index])
        for index, (source, target) in enumerate(
            (
                (dense_gate, wg),
                (dense_up, wu),
                (expert_gate.at[0], eg),
                (expert_up.at[0], eu),
                (expert_down.at[0], ed),
                (dense_down, wd),
            )
        )
    ]
    for load in loads:
        load.start()

    def peer_t(step):
        return lax.rem(me_t + step, tp_count)

    def peer_e(step):
        return lax.rem(me_e + step, ep_count)

    barrier = pltpu.get_barrier_semaphore()
    for step in range(1, tp_count):
        pl.semaphore_signal(
            barrier,
            inc=1,
            device_id=(me_e, peer_t(step)),
            device_id_type=pl.DeviceIdType.MESH,
        )
    for step in range(1, ep_count):
        pl.semaphore_signal(
            barrier,
            inc=1,
            device_id=(peer_e(step), me_t),
            device_id_type=pl.DeviceIdType.MESH,
        )
    pl.semaphore_wait(barrier, tp_count - 1 + ep_count - 1)

    used = [0]
    started = []

    def send(source, target, device):
        index = used[0]
        used[0] = index + 1
        copy = pltpu.make_async_remote_copy(
            src_ref=source,
            dst_ref=target,
            send_sem=send_sem.at[index],
            recv_sem=recv_sem.at[index],
            device_id=device,
            device_id_type=pl.DeviceIdType.MESH,
        )
        copy.start()
        started.append(copy)
        return copy

    def span(index, size):
        return pl.ds(pl.multiple_of(index * size, size), size)

    def dot(left, right):
        return jnp.dot(left, right, preferred_element_type=f32)

    def arrive(copies):
        for copy in copies:
            copy.wait_recv()

    tp_steps = range(1, tp_count)
    ep_steps = range(1, ep_count)
    own = span(me_t, width)

    att = [
        send(part_ref.at[:, span(peer_t(d), width)], att_rx.at[d - 1], (me_e, peer_t(d)))
        for d in tp_steps
    ]
    hots = [
        send(dispatch_ref.at[peer_e(d)], hot.at[me_e], (peer_e(d), me_t)) for d in ep_steps
    ]
    hot[me_e] = dispatch_ref[me_e]
    gain = gain_ref[:, own].astype(f32)
    mix = mix_ref[:, own].astype(f32)
    arrive(att)
    total = part_ref[:, own].astype(f32)
    for d in tp_steps:
        total = total + att_rx[d - 1].astype(f32)
    mid = resid_ref[:, own].astype(f32) + total
    middle[...] = mid
    square = jnp.sum(mid * mid, axis=-1, keepdims=True)
    mixed = jnp.sum(mid * gain * mix, axis=-1, keepdims=True)
    lane = lax.broadcasted_iota(jnp.int32, stat_tx.shape, 1)
    stat = jnp.where(lane < 64, square, mixed)
    stat_tx[...] = stat
    stats = [send(stat_tx, stat_rx.at[d - 1], (me_e, peer_t(d))) for d in tp_steps]
    arrive(stats)
    for d in tp_steps:
        stat = stat + stat_rx[d - 1]
    inverse = lax.rsqrt(stat[:, 0:1] / model_width + EPSILON)
    mixing = jax.nn.sigmoid(inverse * stat[:, 64:65])
    rows[me_e] = (middle[...] * inverse * gain).astype(bf16)

    gathered = [send(rows.at[me_e], rows.at[me_e], (peer_e(d), me_t)) for d in ep_steps]
    arrive(hots)
    arrive(gathered)
    for s in range(ep_count):
        tokens[me_t, s * slots : (s + 1) * slots, :] = dot(hot[s], rows[s]).astype(bf16)
    toks = [send(tokens.at[me_t], tokens.at[me_t], (me_e, peer_t(d))) for d in tp_steps]
    sums = []
    all_rows = rows[...].reshape(ep_count * seq_dev, width)
    for which, weight in enumerate((wg, wu)):
        loads[which].wait()
        gu_tx[which] = dot(all_rows, weight[...]).astype(bf16)
        sums += [
            send(
                gu_tx.at[which, span(peer_t(d), block), :],
                gu_rx.at[which, d - 1],
                (me_e, peer_t(d)),
            )
            for d in tp_steps
        ]
    loads[2].wait()
    loads[3].wait()
    arrive(toks)
    tile = min(256, eg.shape[1])

    def expert_tile(index, carry):
        columns = span(index, tile)
        gate = jnp.zeros((tokens.shape[1], tile), f32)
        up = jnp.zeros((tokens.shape[1], tile), f32)
        for c in range(tp_count):
            features = slice(c * width, (c + 1) * width)
            gate = gate + dot(tokens[c], eg[features, columns])
            up = up + dot(tokens[c], eu[features, columns])
        eh[:, columns] = (jax.nn.silu(gate) * up).astype(bf16)
        return carry

    lax.fori_loop(0, eg.shape[1] // tile, expert_tile, 0)

    arrive(sums)
    gate = gu_tx[0, span(me_t, block), :].astype(f32)
    up = gu_tx[1, span(me_t, block), :].astype(f32)
    for d in tp_steps:
        gate = gate + gu_rx[0, d - 1].astype(f32)
        up = up + gu_rx[1, d - 1].astype(f32)
    mine = span(me_t, block)
    hidden[mine, :] = (jax.nn.silu(gate) * up).astype(bf16)
    hids = [
        send(hidden.at[mine, :], hidden.at[mine, :], (me_e, peer_t(d))) for d in tp_steps
    ]
    loads[4].wait()
    partials = []
    for d in range(1, tp_count + 1):
        target = peer_t(d)
        er_tx[target] = dot(eh[...], ed[:, span(target, width)]).astype(bf16)
        if d < tp_count:
            partials.append(send(er_tx.at[target], er_rx.at[d - 1], (me_e, target)))
    loads[5].wait()
    arrive(hids)
    do_tx[...] = dot(hidden[...], wd[...]).astype(bf16)
    outs = [
        send(do_tx.at[span(peer_e(d), seq_dev), :], do_rx.at[d - 1], (peer_e(d), me_t))
        for d in ep_steps
    ]
    arrive(partials)
    result = er_tx[me_t].astype(f32)
    for d in tp_steps:
        result = result + er_rx[d - 1].astype(f32)
    mo_tx[...] = result.astype(bf16)
    place = span(me_e, slots)
    backs = [
        send(mo_tx.at[span(peer_e(d), slots), :], mo_rx.at[place, :], (peer_e(d), me_t))
        for d in ep_steps
    ]
    mo_rx[place, :] = mo_tx[place, :]
    arrive(outs)
    dense = do_tx[span(me_e, seq_dev), :].astype(f32)
    for d in ep_steps:
        dense = dense + do_rx[d - 1].astype(f32)
    partly = middle[...] + mixing * dense
    arrive(backs)
    out_ref[...] = (partly + dot(combine_ref[...], mo_rx[...])).astype(bf16)
    for copy in started:
        copy.wait_send()


def tail(part, resid, gain, mix, dispatch, combine, weights, tp_count, ep_count):
    seq_dev, model_width = resid.shape
    width = model_width // tp_count
    slots = dispatch.shape[1]
    batch = seq_dev * ep_count
    block = batch // tp_count
    dense_units = weights[0].shape[1]
    expert_units = weights[3].shape[2]
    items = ep_count * slots
    bf16 = jnp.bfloat16
    peers_t = tp_count - 1
    peers_e = ep_count - 1
    copies = 7 * peers_t + 4 * peers_e
    vmem = pl.BlockSpec(memory_space=pltpu.VMEM)
    anywhere = pl.BlockSpec(memory_space=pl.ANY)
    return pl.pallas_call(
        functools.partial(tail_kernel, tp_count, ep_count, slots),
        out_shape=jax.ShapeDtypeStruct((seq_dev, width), bf16),
        in_specs=[vmem] * 6 + [anywhere] * 6,
        out_specs=vmem,
        scratch_shapes=[
            pltpu.VMEM(weights[0].shape, bf16),
            pltpu.VMEM(weights[1].shape, bf16),
            pltpu.VMEM(weights[2].shape, bf16),
            pltpu.VMEM(weights[3].shape[1:], bf16),
            pltpu.VMEM(weights[4].shape[1:], bf16),
            pltpu.VMEM(weights[5].shape[1:], bf16),
            pltpu.VMEM((peers_t, seq_dev, width), bf16),
            pltpu.VMEM((seq_dev, width), jnp.float32),
            pltpu.VMEM((seq_dev, 128), jnp.float32),
            pltpu.VMEM((peers_t, seq_dev, 128), jnp.float32),
            pltpu.VMEM((ep_count, seq_dev, width), bf16),
            pltpu.VMEM((ep_count, slots, seq_dev), bf16),
            pltpu.VMEM((tp_count, items, width), bf16),
            pltpu.VMEM((2, batch, dense_units), bf16),
            pltpu.VMEM((2, peers_t, block, dense_units), bf16),
            pltpu.VMEM((batch, dense_units), bf16),
            pltpu.VMEM((items, expert_units), bf16),
            pltpu.VMEM((tp_count, items, width), bf16),
            pltpu.VMEM((peers_t, items, width), bf16),
            pltpu.VMEM((batch, width), bf16),
            pltpu.VMEM((peers_e, seq_dev, width), bf16),
            pltpu.VMEM((items, width), bf16),
            pltpu.VMEM((items, width), bf16),
            pltpu.SemaphoreType.DMA((6,)),
            pltpu.SemaphoreType.DMA((copies,)),
            pltpu.SemaphoreType.DMA((copies,)),
        ],
        compiler_params=pltpu.CompilerParams(
            collective_id=0, has_side_effects=True, vmem_limit_bytes=40 * 1024 * 1024
        ),
        name="tail",
    )(part, resid, gain, mix, dispatch, combine, *weights)


def per_device(
    resid,
    norm_gain,
    w_query,
    w_key,
    w_value,
    w_gate,
    head_gain,
    w_output,
    state,
    positions,
    ffn_gain,
    w_mix,
    dense_gate,
    dense_up,
    dense_down,
    routes,
    route_weight,
    expert_gate,
    expert_up,
    expert_down,
):
    seq_dev = resid.shape[0]
    tp_count = lax.axis_size("tp")
    ep_count = lax.axis_size("ep")
    tp_index = lax.axis_index("tp")
    normed_in = rms_norm(resid.astype(jnp.float32), norm_gain).astype(jnp.bfloat16)

    def project(weight):
        return jnp.dot(normed_in, weight, preferred_element_type=jnp.float32).astype(jnp.bfloat16)

    heads_here = state.shape[1]
    head_first = (tp_index * heads_here).astype(jnp.float32)
    retained, new_state = retain(
        project(w_query),
        project(w_key),
        project(w_value),
        project(w_gate),
        state,
        positions,
        head_first,
        head_gain,
    )
    part = jnp.dot(retained, w_output, preferred_element_type=jnp.float32).astype(jnp.bfloat16)
    top_count = routes.shape[1]
    capacity = max(2, 2 * seq_dev * top_count // ep_count)
    slots = -(-capacity // 16) * 16
    dispatch, combine = routing(routes, route_weight, capacity, slots, ep_count)
    final = tail(
        part,
        resid,
        ffn_gain[None, :],
        w_mix[None, :],
        dispatch,
        combine,
        (dense_gate, dense_up, dense_down, expert_gate, expert_up, expert_down),
        tp_count,
        ep_count,
    )
    return (final, new_state)


def solution(mesh):
    in_specs = (
        P("ep", None),
        P(),
        P(None, "tp"),
        P(None, "tp"),
        P(None, "tp"),
        P(None, "tp"),
        P("tp"),
        P("tp", None),
        P("ep", "tp", None, None),
        P("ep"),
        P(),
        P(),
        P("tp", "ep"),
        P("tp", "ep"),
        P("ep", "tp"),
        P("ep", None),
        P("ep", None),
        P("ep", None, "tp"),
        P("ep", None, "tp"),
        P("ep", "tp", None),
    )
    out_specs = (P("ep", "tp"), P("ep", "tp", None, None))
    return jax.shard_map(
        per_device, mesh=mesh, in_specs=in_specs, out_specs=out_specs, check_vma=False
    )
```

time: 235 us -> 84.9 us (0.36)
  the two profiles are of different devices: /device:TPU:0 before, /device:TPU:1 now
where the time goes in v1:
time: 84.9 us; the launch traced here: 84.4 us
  Pallas kernels  51.3 us (60%)
  matrix products  11.8 us (14%)
  local copies, waits for them, and re-layouts  11.3 us (13%)
  other arithmetic  9.13 us (11%)
  between operations  0.92 us (1%)
    pallas_call x1, Pallas kernels, tail(): pl.pallas_call(functools.partial(tail_kernel, tp_count, ep_count, slots),...  51.3 us
    unnamed x28, local copies, waits for them, and re-layouts  9.46 us
    dot_general x1, matrix products, retain(): jnp.einsum('shd,shde->she', query_rot, memory, precision=lax.Precision.HI...  5.35 us
    dot_general x3, matrix products, project(): jnp.dot(normed_in, weight, preferred_element_type=jnp.float32)  4.96 us
    add x1, other arithmetic, retain(): decays[None, :, None, None] * memory  3.09 us

profile of v1, /device:TPU:1, one launch (start us, length us, event | category | flops | bytes accessed | tf_op | source)
XLA Modules:
  0.0 84.4 jit_solution(13432657699482623647)
XLA Ops:
  0.7 0.7 convert_element_type.65
  1.4 1.0 %fusion.7 = f32[32]{0:T(128)S(1)} fusion(bf16[32,2048]{1,0:T(8,128)(2,1)} %resid_ref.1), kind=kLoop, calls=%fused_computation.15 | loop fusion | flops 196576 | bytes 131200 | tf_op jit(solution)/shard_map/reduce_sum | solution.py:15
  2.5 0.7 convert_element_type.69
  3.1 0.7 convert_element_type.75
  3.8 0.7 convert_element_type.60
  4.5 0.7 broadcast_in_dim.12.gain_ref
  5.2 0.7 broadcast_in_dim.13.mix_ref
  5.9 0.8 copy.42
  7.1 0.2 select_reduce_fusion.1
  7.4 0.7 multiply_add_fusion.3
  8.4 1.6 %fusion.5 = f32[32,256]{1,0:T(8,128)S(1)} fusion(bf16[2048,256]{1,0:T(8,128)(2,1)} %param.22, bf16[32,2048]{1,0:T(8,128)(2,1)} %resid_ref.1, f32[2048]{0:T(1024)S(1)} %convert_element_type.60, f32[32]{0:T(128)S(1)} %add_rsqrt_fusion.1), kind=kOutput, calls=%fused_computation.10 | convolution fusion | flops 33832960 | bytes 1220736 | tf_op jit(solution)/shard_map/dot_general | solution.py:398
  10.1 1.7 %fusion.4 = f32[32,256]{1,0:T(8,128)S(1)} fusion(bf16[2048,256]{1,0:T(8,128)(2,1)} %param.23, bf16[32,2048]{1,0:T(8,128)(2,1)} %resid_ref.1, f32[2048]{0:T(1024)S(1)} %convert_element_type.60, f32[32]{0:T(128)S(1)} %add_rsqrt_fusion.1), kind=kOutput, calls=%fused_computation.8 | convolution fusion | flops 33832960 | bytes 1220736 | tf_op jit(solution)/shard_map/dot_general | solution.py:398
  11.8 1.6 %fusion.3 = f32[32,256]{1,0:T(8,128)S(1)} fusion(bf16[2048,256]{1,0:T(8,128)(2,1)} %param.24, bf16[32,2048]{1,0:T(8,128)(2,1)} %resid_ref.1, f32[2048]{0:T(1024)S(1)} %convert_element_type.60, f32[32]{0:T(128)S(1)} %add_rsqrt_fusion.1), kind=kOutput, calls=%fused_computation.6 | convolution fusion | flops 33832960 | bytes 1220736 | tf_op jit(solution)/shard_map/dot_general | solution.py:398
  13.8 5.4 %fusion.24 = f32[32,2,1,128]{3,2,1,0:T(1,128)S(1)} fusion(f32[32,2,128,1]{2,3,1,0:T(1,128)S(1)} %bitcast.24, f32[32,2,128,128]{3,2,1,0:T(8,128)} %param.28), kind=kOutput, calls=%fused_computation.50 | convolution fusion | flops 12582912 | bytes 4259840 | tf_op jit(solution)/shard_map/shd,shde->she/dot_general | solution.py:44
  19.2 0.2 fusion.23
  19.8 1.5 %convolution_convert_fusion.part_ref = bf16[32,2048]{1,0:T(8,128)(2,1)} fusion(bf16[256,2048]{1,0:T(8,128)(2,1)S(1)} %copy-done, f32[4,8,2,128]{3,2,1,0:T(2,128)S(1)} %bitcast.23, bf16[2048,256]{1,0:T(8,128)(2,1)S(1)} %copy-done.7, f32[256]{0:T(256)S(1)} %convert_element_type.69, bf16[32,2048]{1,0:T(8,128)(2,1)S(1)} %copy-done.1, ...), kind=kOutput, calls=%fused_computation.2 | convolution fusion | flops 67510272 | bytes 2401408 | tf_op jit(solution)/shard_map/dot_general | solution.py:412
  21.3 1.4 %copy.45.dense_gate = bf16[512,704]{1,0:T(8,128)(2,1)S(1)} copy(bf16[512,704]{0,1:T(8,128)(2,1)} %param.32) | data formatting | bytes 1441792 | tf_op args[12]
  22.7 1.4 %copy.46.dense_up = bf16[512,704]{1,0:T(8,128)(2,1)S(1)} copy(bf16[512,704]{0,1:T(8,128)(2,1)} %param.33) | data formatting | bytes 1441792 | tf_op args[13]
  24.1 2.2 %copy-done.2 = bf16[1,2048,1024]{2,1,0:T(8,128)(2,1)S(1)} copy-done((bf16[1,2048,1024]{2,1,0:T(8,128)(2,1)S(1)}, bf16[1,2048,1024]{2,1,0:T(8,128)(2,1)}, u32[]{:S(2)}) %copy-start.2) | copy-done | bytes 4194328
  26.3 2.2 %copy-done.3 = bf16[1,2048,1024]{2,1,0:T(8,128)(2,1)S(1)} copy-done((bf16[1,2048,1024]{2,1,0:T(8,128)(2,1)S(1)}, bf16[1,2048,1024]{2,1,0:T(8,128)(2,1)}, u32[]{:S(2)}) %copy-start.3) | copy-done | bytes 4194328
  28.5 0.9 %copy-done.5 = bf16[32,2048]{1,0:T(8,128)(2,1)S(1)} copy-done((bf16[32,2048]{1,0:T(8,128)(2,1)S(1)}, bf16[32,2048]{1,0:T(8,128)(2,1)}, u32[]{:S(2)}) %copy-start.5) | copy-done | bytes 131096
  29.4 51.3 %tail.1 = bf16[32,512]{1,0:T(8,128)(2,1)S(1)} custom-call(bf16[32,2048]{1,0:T(8,128)(2,1)S(1)} %copy-done.5, bf16[32,2048]{1,0:T(8,128)(2,1)S(1)} %copy-done.1, bf16[1,2048]{1,0:T(2,128)(2,1)S(1)} %broadcast_in_dim.12.gain_ref, bf16[1,2048]{1,0:T(2,128)(2,1)S(1)} %broadcast_in_dim.13.mix_ref, bf16[8,16,32]{2,1,0:T(8,128)(2,1)S(1)} %bitcast.22, ...), custom_call_target="tpu_custom_call" | custom-call | tf_op jit(solution)/shard_map/tail/pallas_call | solution.py:329
  80.7 3.1 %multiply_add_fusion = f32[32,2,128,128]{3,2,1,0:T(8,128)} fusion(f32[32,2,128,128]{3,2,1,0:T(8,128)S(1)} %copy-done.6, f32[32,2,128]{2,1,0:T(2,128)S(1)} %copy-done.9, f32[32,2,128]{2,1,0:T(2,128)S(1)} %copy-done.11, f32[2]{0:T(128)S(1)} %exponential_subtract_fusion), kind=kLoop, calls=%fused_computation.1 | loop fusion | flops 3145728 | bytes 8454152 | tf_op jit(solution)/shard_map/add | solution.py:49
  83.8 0.6 copy.54
  (43 shorter events, 1.7 us)
Async XLA Ops:
  0.6 19.2 %copy-start = (bf16[256,2048]{1,0:T(8,128)(2,1)S(1)}, bf16[256,2048]{1,0:T(8,128)(2,1)}, u32[]{:S(2)}) copy-start(bf16[256,2048]{1,0:T(8,128)(2,1)} %param.27) | copy-start | bytes 3145732
  10.1 9.8 %copy-start.1 = (bf16[32,2048]{1,0:T(8,128)(2,1)S(1)}, bf16[32,2048]{1,0:T(8,128)(2,1)}, u32[]{:S(2)}) copy-start(bf16[32,2048]{1,0:T(8,128)(2,1)} %resid_ref.1) | copy-start | bytes 393220
  10.1 9.8 %copy-start.7 = (bf16[2048,256]{1,0:T(8,128)(2,1)S(1)}, bf16[2048,256]{1,0:T(8,128)(2,1)}, u32[]{:S(2)}) copy-start(bf16[2048,256]{1,0:T(8,128)(2,1)} %param.25) | copy-start | bytes 3145732
  13.5 6.1 %copy-start.8 = (f32[32,2,128]{2,1,0:T(2,128)}, f32[32,2,128]{2,1,0:T(2,128)S(1)}, u32[]{:S(2)}) copy-start(f32[32,2,128]{2,1,0:T(2,128)S(1)} %reshape.164) | copy-start | bytes 98308
  13.8 6.0 %copy-start.10 = (f32[32,2,128]{2,1,0:T(2,128)}, f32[32,2,128]{2,1,0:T(2,128)S(1)}, u32[]{:S(2)}) copy-start(f32[32,2,128]{2,1,0:T(2,128)S(1)} %get-tuple-element.13) | copy-start | bytes 98308
  13.8 10.2 %copy-start.4 = (bf16[704,512]{1,0:T(8,128)(2,1)S(1)}, bf16[704,512]{1,0:T(8,128)(2,1)}, u32[]{:S(2)}) copy-start(bf16[704,512]{1,0:T(8,128)(2,1)} %dense_down.1) | copy-start | bytes 2162692
  24.1 2.2 %copy-start.2 = (bf16[1,2048,1024]{2,1,0:T(8,128)(2,1)S(1)}, bf16[1,2048,1024]{2,1,0:T(8,128)(2,1)}, u32[]{:S(2)}) copy-start(bf16[1,2048,1024]{2,1,0:T(8,128)(2,1)} %expert_gate.1) | copy-start | bytes 12582916
  26.3 2.2 %copy-start.3 = (bf16[1,2048,1024]{2,1,0:T(8,128)(2,1)S(1)}, bf16[1,2048,1024]{2,1,0:T(8,128)(2,1)}, u32[]{:S(2)}) copy-start(bf16[1,2048,1024]{2,1,0:T(8,128)(2,1)} %expert_up.1) | copy-start | bytes 12582916
  28.5 0.9 %copy-start.5 = (bf16[32,2048]{1,0:T(8,128)(2,1)S(1)}, bf16[32,2048]{1,0:T(8,128)(2,1)}, u32[]{:S(2)}) copy-start(bf16[32,2048]{1,0:T(8,128)(2,1)} %convolution_convert_fusion.part_ref) | copy-start | bytes 393220
  29.4 51.3 %copy-start.6 = (f32[32,2,128,128]{3,2,1,0:T(8,128)S(1)}, f32[32,2,128,128]{3,2,1,0:T(8,128)}, u32[]{:S(2)}) copy-start(f32[32,2,128,128]{3,2,1,0:T(8,128)} %param.28) | copy-start | bytes 12582916
  29.4 51.3 %copy-start.9 = (f32[32,2,128]{2,1,0:T(2,128)S(1)}, f32[32,2,128]{2,1,0:T(2,128)}, u32[]{:S(2)}) copy-start(f32[32,2,128]{2,1,0:T(2,128)} %copy-done.8) | copy-start | bytes 98308
  29.4 51.3 %copy-start.11 = (f32[32,2,128]{2,1,0:T(2,128)S(1)}, f32[32,2,128]{2,1,0:T(2,128)}, u32[]{:S(2)}) copy-start(f32[32,2,128]{2,1,0:T(2,128)} %copy-done.10) | copy-start | bytes 98308

commit v2 on v1

--- a/solution.py
+++ b/solution.py
@@ -81,8 +81,7 @@
     slots,
     part_ref,
     resid_ref,
-    gain_ref,
-    mix_ref,
+    scale_ref,
     dispatch_ref,
     combine_ref,
     dense_gate,
@@ -107,10 +106,14 @@
     tokens,
     gu_tx,
     gu_rx,
+    gu_pair,
+    gu_far,
     hidden,
     eh,
     er_tx,
     er_rx,
+    er_pair,
+    er_far,
     do_tx,
     do_rx,
     mo_tx,
@@ -194,6 +197,26 @@
         for copy in copies:
             copy.wait_recv()
 
+    half = tp_count // 2
+    sibling = me_t + 1 - 2 * lax.rem(me_t, 2)
+
+    def across(index, step):
+        return lax.rem(index + 2 * step, tp_count)
+
+    def spread(at):
+        return [
+            send(at(me_t), at(me_t), (me_e, target))
+            for target in [sibling] + [across(me_t, k) for k in range(1, half)]
+        ]
+
+    def pass_on(copies, at):
+        waiting = [copies[0]]
+        for k in range(1, half):
+            copies[k].wait_recv()
+            origin = across(me_t, half - k)
+            waiting.append(send(at(origin), at(origin), (me_e, sibling)))
+        return waiting
+
     tp_steps = range(1, tp_count)
     ep_steps = range(1, ep_count)
     own = span(me_t, width)
@@ -206,8 +229,9 @@
         send(dispatch_ref.at[peer_e(d)], hot.at[me_e], (peer_e(d), me_t)) for d in ep_steps
     ]
     hot[me_e] = dispatch_ref[me_e]
-    gain = gain_ref[:, own].astype(f32)
-    mix = mix_ref[:, own].astype(f32)
+    scales = scale_ref[:, own].astype(f32)
+    gain = scales[0:1, :]
+    mix = scales[1:2, :]
     arrive(att)
     total = part_ref[:, own].astype(f32)
     for d in tp_steps:
@@ -232,20 +256,36 @@
     arrive(gathered)
     for s in range(ep_count):
         tokens[me_t, s * slots : (s + 1) * slots, :] = dot(hot[s], rows[s]).astype(bf16)
-    toks = [send(tokens.at[me_t], tokens.at[me_t], (me_e, peer_t(d))) for d in tp_steps]
-    sums = []
+    toks = spread(lambda index: tokens.at[index])
+    near = []
     all_rows = rows[...].reshape(ep_count * seq_dev, width)
     for which, weight in enumerate((wg, wu)):
         loads[which].wait()
-        gu_tx[which] = dot(all_rows, weight[...]).astype(bf16)
-        sums += [
-            send(
-                gu_tx.at[which, span(peer_t(d), block), :],
-                gu_rx.at[which, d - 1],
-                (me_e, peer_t(d)),
+        gu_tx[which] = lax.dot_general(
+            all_rows, weight[...], (((1,), (1,)), ((), ())), preferred_element_type=f32
+        ).astype(bf16)
+        near.append(
+            [
+                send(
+                    gu_tx.at[which, span(across(sibling, k), block), :],
+                    gu_rx.at[which, k],
+                    (me_e, sibling),
+                )
+                for k in range(half)
+            ]
+        )
+    toks = pass_on(toks, lambda index: tokens.at[index])
+    far = []
+    for which in range(2):
+        arrive(near[which])
+        for k in range(1, half):
+            target = across(me_t, k)
+            gu_pair[which, k - 1] = (
+                gu_tx[which, span(target, block), :].astype(f32) + gu_rx[which, k].astype(f32)
+            ).astype(bf16)
+            far.append(
+                send(gu_pair.at[which, k - 1], gu_far.at[which, k - 1], (me_e, target))
             )
-            for d in tp_steps
-        ]
     loads[2].wait()
     loads[3].wait()
     arrive(toks)
@@ -264,24 +304,28 @@
 
     lax.fori_loop(0, eg.shape[1] // tile, expert_tile, 0)
 
-    arrive(sums)
-    gate = gu_tx[0, span(me_t, block), :].astype(f32)
-    up = gu_tx[1, span(me_t, block), :].astype(f32)
-    for d in tp_steps:
-        gate = gate + gu_rx[0, d - 1].astype(f32)
-        up = up + gu_rx[1, d - 1].astype(f32)
-    mine = span(me_t, block)
-    hidden[mine, :] = (jax.nn.silu(gate) * up).astype(bf16)
-    hids = [
-        send(hidden.at[mine, :], hidden.at[mine, :], (me_e, peer_t(d))) for d in tp_steps
-    ]
+    arrive(far)
+    gate = gu_tx[0, span(me_t, block), :].astype(f32) + gu_rx[0, 0].astype(f32)
+    up = gu_tx[1, span(me_t, block), :].astype(f32) + gu_rx[1, 0].astype(f32)
+    for k in range(1, half):
+        gate = gate + gu_far[0, k - 1].astype(f32)
+        up = up + gu_far[1, k - 1].astype(f32)
+    hidden[span(me_t, block), :] = (jax.nn.silu(gate) * up).astype(bf16)
+    hids = spread(lambda index: hidden.at[span(index, block), :])
     loads[4].wait()
+    pairs = []
+    for k in range(half):
+        target = across(sibling, k)
+        er_tx[k] = dot(eh[...], ed[:, span(target, width)]).astype(bf16)
+        pairs.append(send(er_tx.at[k], er_rx.at[k], (me_e, sibling)))
+    hids = pass_on(hids, lambda index: hidden.at[span(index, block), :])
     partials = []
-    for d in range(1, tp_count + 1):
-        target = peer_t(d)
-        er_tx[target] = dot(eh[...], ed[:, span(target, width)]).astype(bf16)
-        if d < tp_count:
-            partials.append(send(er_tx.at[target], er_rx.at[d - 1], (me_e, target)))
+    for k in range(1, half):
+        target = across(me_t, k)
+        summed = dot(eh[...], ed[:, span(target, width)])
+        arrive(pairs[k : k + 1])
+        er_pair[k - 1] = (summed + er_rx[k].astype(f32)).astype(bf16)
+        partials.append(send(er_pair.at[k - 1], er_far.at[k - 1], (me_e, target)))
     loads[5].wait()
     arrive(hids)
     do_tx[...] = dot(hidden[...], wd[...]).astype(bf16)
@@ -289,10 +333,12 @@
         send(do_tx.at[span(peer_e(d), seq_dev), :], do_rx.at[d - 1], (peer_e(d), me_t))
         for d in ep_steps
     ]
+    result = dot(eh[...], ed[:, own])
+    arrive(pairs[:1])
+    result = result + er_rx[0].astype(f32)
     arrive(partials)
-    result = er_tx[me_t].astype(f32)
-    for d in tp_steps:
-        result = result + er_rx[d - 1].astype(f32)
+    for k in range(1, half):
+        result = result + er_far[k - 1].astype(f32)
     mo_tx[...] = result.astype(bf16)
     place = span(me_e, slots)
     backs = [
@@ -311,13 +357,14 @@
         copy.wait_send()
 
 
-def tail(part, resid, gain, mix, dispatch, combine, weights, tp_count, ep_count):
+def tail(part, resid, scale, dispatch, combine, weights, tp_count, ep_count):
     seq_dev, model_width = resid.shape
     width = model_width // tp_count
     slots = dispatch.shape[1]
     batch = seq_dev * ep_count
     block = batch // tp_count
-    dense_units = weights[0].shape[1]
+    dense_units = weights[0].shape[0]
+    half = tp_count // 2
     expert_units = weights[3].shape[2]
     items = ep_count * slots
     bf16 = jnp.bfloat16
@@ -325,11 +372,11 @@
     peers_e = ep_count - 1
     copies = 7 * peers_t + 4 * peers_e
     vmem = pl.BlockSpec(memory_space=pltpu.VMEM)
-    anywhere = pl.BlockSpec(memory_space=pl.ANY)
+    anywhere = pl.BlockSpec(memory_space=pltpu.HBM)
     return pl.pallas_call(
         functools.partial(tail_kernel, tp_count, ep_count, slots),
         out_shape=jax.ShapeDtypeStruct((seq_dev, width), bf16),
-        in_specs=[vmem] * 6 + [anywhere] * 6,
+        in_specs=[vmem] * 5 + [anywhere] * 6,
         out_specs=vmem,
         scratch_shapes=[
             pltpu.VMEM(weights[0].shape, bf16),
@@ -346,11 +393,15 @@
             pltpu.VMEM((ep_count, slots, seq_dev), bf16),
             pltpu.VMEM((tp_count, items, width), bf16),
             pltpu.VMEM((2, batch, dense_units), bf16),
-            pltpu.VMEM((2, peers_t, block, dense_units), bf16),
+            pltpu.VMEM((2, half, block, dense_units), bf16),
+            pltpu.VMEM((2, half - 1, block, dense_units), bf16),
+            pltpu.VMEM((2, half - 1, block, dense_units), bf16),
             pltpu.VMEM((batch, dense_units), bf16),
             pltpu.VMEM((items, expert_units), bf16),
-            pltpu.VMEM((tp_count, items, width), bf16),
-            pltpu.VMEM((peers_t, items, width), bf16),
+            pltpu.VMEM((half, items, width), bf16),
+            pltpu.VMEM((half, items, width), bf16),
+            pltpu.VMEM((half - 1, items, width), bf16),
+            pltpu.VMEM((half - 1, items, width), bf16),
             pltpu.VMEM((batch, width), bf16),
             pltpu.VMEM((peers_e, seq_dev, width), bf16),
             pltpu.VMEM((items, width), bf16),
@@ -360,10 +411,10 @@
             pltpu.SemaphoreType.DMA((copies,)),
         ],
         compiler_params=pltpu.CompilerParams(
-            collective_id=0, has_side_effects=True, vmem_limit_bytes=40 * 1024 * 1024
+            collective_id=0, has_side_effects=True, vmem_limit_bytes=61 * 1024 * 1024
         ),
         name="tail",
-    )(part, resid, gain, mix, dispatch, combine, *weights)
+    )(part, resid, scale, dispatch, combine, *weights)
 
 
 def per_device(
@@ -417,11 +468,10 @@
     final = tail(
         part,
         resid,
-        ffn_gain[None, :],
-        w_mix[None, :],
+        jnp.stack([ffn_gain, w_mix]),
         dispatch,
         combine,
-        (dense_gate, dense_up, dense_down, expert_gate, expert_up, expert_down),
+        (dense_gate.T, dense_up.T, dense_down, expert_gate, expert_up, expert_down),
         tp_count,
         ep_count,
     )

time: 84.9 us -> 74.1 us (0.87)
  the two profiles are of different devices: /device:TPU:1 before, /device:TPU:0 now
where the time goes in v2:
time: 74.1 us; the launch traced here: 72.7 us
  Pallas kernels  44.9 us (61%)
  matrix products  11.7 us (16%)
  other arithmetic  11.5 us (16%)
  local copies, waits for them, and re-layouts  3.85 us (5%)
  between operations  0.82 us (1%)
    pallas_call x1, Pallas kernels, tail(): pl.pallas_call(functools.partial(tail_kernel, tp_count, ep_count, slots),...  44.9 us
    dot_general x1, matrix products, retain(): jnp.einsum('shd,shde->she', query_rot, memory, precision=lax.Precision.HI...  5.28 us
    dot_general x3, matrix products, project(): jnp.dot(normed_in, weight, preferred_element_type=jnp.float32)  4.95 us
    add x1, other arithmetic, retain(): decays[None, :, None, None] * memory  4.25 us

profile of v2, /device:TPU:0, one launch (start us, length us, event | category | flops | bytes accessed | tf_op | source)
XLA Modules:
  0.0 72.7 jit_solution(13725866249245227797)
XLA Ops:
  0.7 0.7 %convert_element_type.65 = f32[32]{0:T(128)S(1)} convert(s32[32]{0:T(128)} %param.29) | non-fusion elementwise | flops 32 | bytes 256 | tf_op jit(solution)/shard_map/convert_element_type | solution.py:22
  1.4 1.0 %fusion.7 = f32[32]{0:T(128)S(1)} fusion(bf16[32,2048]{1,0:T(8,128)(2,1)} %resid_ref.1), kind=kLoop, calls=%fused_computation.15 | loop fusion | flops 196576 | bytes 131200 | tf_op jit(solution)/shard_map/reduce_sum | solution.py:15
  2.5 0.7 convert_element_type.69
  3.1 0.7 convert_element_type.75
  3.8 0.7 convert_element_type.60
  4.5 0.7 stack.9
  5.2 0.7 stack.10
  5.9 0.6 pad_maximum_fusion.1.scale_ref
  6.5 0.8 %copy.36 = s32[32,2]{1,0:T(8,128)S(1)} copy(s32[32,2]{0,1:T(2,128)} %param.35) | data formatting | bytes 512 | tf_op args[15]
  7.7 0.2 select_reduce_fusion.1
  8.0 0.7 multiply_add_fusion.3
  8.8 0.7 select_reduce_fusion.combine_ref
  9.5 0.7 copy.38
  10.2 1.6 %fusion.5 = f32[32,256]{1,0:T(8,128)S(1)} fusion(bf16[2048,256]{1,0:T(8,128)(2,1)} %param.22, bf16[32,2048]{1,0:T(8,128)(2,1)} %resid_ref.1, f32[2048]{0:T(1024)S(1)} %convert_element_type.60, f32[32]{0:T(128)S(1)} %add_rsqrt_fusion.1), kind=kOutput, calls=%fused_computation.10 | convolution fusion | flops 33832960 | bytes 1220736 | tf_op jit(solution)/shard_map/dot_general | solution.py:449
  11.9 1.7 %fusion.4 = f32[32,256]{1,0:T(8,128)S(1)} fusion(bf16[2048,256]{1,0:T(8,128)(2,1)} %param.23, bf16[32,2048]{1,0:T(8,128)(2,1)} %resid_ref.1, f32[2048]{0:T(1024)S(1)} %convert_element_type.60, f32[32]{0:T(128)S(1)} %add_rsqrt_fusion.1), kind=kOutput, calls=%fused_computation.8 | convolution fusion | flops 33832960 | bytes 1220736 | tf_op jit(solution)/shard_map/dot_general | solution.py:449
  13.6 1.6 %fusion.3 = f32[32,256]{1,0:T(8,128)S(1)} fusion(bf16[2048,256]{1,0:T(8,128)(2,1)} %param.24, bf16[32,2048]{1,0:T(8,128)(2,1)} %resid_ref.1, f32[2048]{0:T(1024)S(1)} %convert_element_type.60, f32[32]{0:T(128)S(1)} %add_rsqrt_fusion.1), kind=kOutput, calls=%fused_computation.6 | convolution fusion | flops 33832960 | bytes 1220736 | tf_op jit(solution)/shard_map/dot_general | solution.py:449
  15.3 0.2 multiply_subtract_fusion
  15.6 5.3 %fusion.24 = f32[32,2,1,128]{3,2,1,0:T(1,128)S(1)} fusion(f32[32,2,128,1]{2,3,1,0:T(1,128)S(1)} %bitcast.28, f32[32,2,128,128]{3,2,1,0:T(8,128)} %param.28), kind=kOutput, calls=%fused_computation.51 | convolution fusion | flops 12582912 | bytes 4259840 | tf_op jit(solution)/shard_map/shd,shde->she/dot_general | solution.py:44
  20.9 0.2 fusion.23
  21.2 0.2 multiply_reduce_fusion
  21.5 1.5 %convolution_convert_fusion.part_ref = bf16[32,2048]{1,0:T(8,128)(2,1)} fusion(bf16[256,2048]{1,0:T(8,128)(2,1)S(1)} %copy-done, f32[4,8,2,128]{3,2,1,0:T(2,128)S(1)} %bitcast.26, bf16[2048,256]{1,0:T(8,128)(2,1)S(1)} %copy-done.2, f32[256]{0:T(256)S(1)} %convert_element_type.69, bf16[32,2048]{1,0:T(8,128)(2,1)S(1)} %copy-done.1, ...), kind=kOutput, calls=%fused_computation.2 | convolution fusion | flops 67510272 | bytes 2401408 | tf_op jit(solution)/shard_map/dot_general | solution.py:463
  23.0 44.9 %tail.1 = bf16[32,512]{1,0:T(8,128)(2,1)} custom-call(bf16[32,2048]{1,0:T(8,128)(2,1)} %convolution_convert_fusion.part_ref, bf16[32,2048]{1,0:T(8,128)(2,1)} %resid_ref.1, bf16[2,2048]{1,0:T(2,128)(2,1)} %pad_maximum_fusion.1.scale_ref, bf16[8,16,32]{2,1,0:T(8,128)(2,1)} %bitcast.27, bf16[32,128]{1,0:T(8,128)(2,1)} %select_reduce_fusion.combine_ref, ...), custom_call_target="tpu_custom_call" | custom-call | tf_op jit(solution)/shard_map/tail/pallas_call | solution.py:376
  67.9 4.2 %multiply_add_fusion = f32[32,2,128,128]{3,2,1,0:T(8,128)} fusion(f32[32,2,128,128]{3,2,1,0:T(8,128)} %param.28, f32[32,2,128]{2,1,0:T(2,128)S(1)} %reshape.164, f32[32,2,128]{2,1,0:T(2,128)S(1)} %get-tuple-element.13, f32[2]{0:T(128)S(1)} %exponential_subtract_fusion), kind=kLoop, calls=%fused_computation.1 | loop fusion | flops 3145728 | bytes 8454152 | tf_op jit(solution)/shard_map/add | solution.py:49
  72.1 0.6 copy.46
  (26 shorter events, 1.1 us)
Async XLA Ops:
  0.6 20.9 %copy-start = (bf16[256,2048]{1,0:T(8,128)(2,1)S(1)}, bf16[256,2048]{1,0:T(8,128)(2,1)}, u32[]{:S(2)}) copy-start(bf16[256,2048]{1,0:T(8,128)(2,1)} %param.27) | copy-start | bytes 3145732
  11.9 9.6 %copy-start.1 = (bf16[32,2048]{1,0:T(8,128)(2,1)S(1)}, bf16[32,2048]{1,0:T(8,128)(2,1)}, u32[]{:S(2)}) copy-start(bf16[32,2048]{1,0:T(8,128)(2,1)} %resid_ref.1) | copy-start | bytes 393220
  11.9 9.6 %copy-start.2 = (bf16[2048,256]{1,0:T(8,128)(2,1)S(1)}, bf16[2048,256]{1,0:T(8,128)(2,1)}, u32[]{:S(2)}) copy-start(bf16[2048,256]{1,0:T(8,128)(2,1)} %param.25) | copy-start | bytes 3145732
  67.9 4.3 %copy-start.3 = (bf16[32,512]{1,0:T(8,128)(2,1)S(1)}, bf16[32,512]{1,0:T(8,128)(2,1)}, u32[]{:S(2)}) copy-start(bf16[32,512]{1,0:T(8,128)(2,1)} %tail.1) | copy-start | bytes 98308
